TPU v7x, 32 devices: a whole 2x2x4 slice. The times are simulated.
32 devices in a mesh: grp: 2 (over x), st: 4 (over y, core), tp: 4 (over z).
Axes of the slice: x: 2, y: 2, z: 4, core: 2. Of those that a mesh axis runs over, the one named last changes fastest.
Arguments:
- tokens: bfloat16 [4096, 2048], P(('grp', 'st')), parts along dimension 0, may hold values from -6 to 6, as said below
- store: bfloat16 [64, 128, 2048], P(('grp', 'st')), parts along dimension 0, may hold values from -6 to 6, as said below
- passage_ids: int32 [64, 4], P(('grp', 'st')), parts along dimension 0, may hold values from 0 to 31, as said below
- mix_gain: float32 [2048], replicated, may hold values from 0.1 to 1.9
- glu_value: bfloat16 [2048, 1024], P(None, 'tp'), may hold values from -0.125 to 0.125
- glu_gate: bfloat16 [2048, 1024], P(None, 'tp'), may hold values from -0.125 to 0.125
- conv_taps: bfloat16 [31, 1024], P(None, 'tp'), may hold values from -5 to 5
- channel_gain: float32 [1024], P('tp'), may hold values from 0.1 to 1.9
- mix_out: bfloat16 [1024, 2048], P('tp'), may hold values from -0.1875 to 0.1875
- query_gain: float32 [2048], replicated, may hold values from 0.1 to 1.9
- passage_gain: float32 [2048], replicated, may hold values from 0.1 to 1.9
- query_proj: bfloat16 [2048, 2048], P(None, 'tp'), may hold values from -1 to 1
- key_proj: bfloat16 [2048, 2048], P(None, 'tp'), may hold values from -1 to 1
- value_proj: bfloat16 [2048, 2048], P(None, 'tp'), may hold values from -0.125 to 0.125
- attn_out: bfloat16 [2048, 2048], P('tp'), may hold values from -0.125 to 0.125
- blend_gain: float32 [2048], replicated, may hold values from 0.5 to 3
Outputs:
- blended: bfloat16 [4096, 2048], P(('grp', 'st', 'tp')), parts along dimension 0
There are 2 independent parts, one for each index of `grp`. A program takes and returns all parts, laid end to end along the dimension named above; an argument that names none is the same for every part. Nothing has to cross between parts.
Inputs may be any that keep to these rules, and one draw needn't show every extreme that they name: `tokens`: standard normal entries clipped to the range. `store`: standard normal entries clipped to the range. `passage_ids`: passage p is held by index p // 8 of st. The 32 requests of the 8 blocks of one index of st (repeats counted) name at most 16 passages held by any one index of st, and in every draw one index of st receives exactly 16 requests from every index of st.
All inputs are finite; a program needn't handle non-finite values.
Results may differ from a plain program's by a relative error of at most 0.01575.
The roundings to bfloat16 on the way count: a program that leaves them out, or rounds other values in their place, can miss the bound.
Values may be sent and summed in bfloat16 or wider, within the bound.
A program may use at most 128 MiB of HBM per device.

v0:
```python
import jax
import jax.numpy as jnp
from jax import lax
from jax.sharding import PartitionSpec as P

CA = 1024
HD = 256
SEQ_LEN = 128


EPS = 1e-06


def rms_rows(row_data, gain_vec):
    floats = row_data.astype(jnp.float32)
    inv_scale = lax.rsqrt(jnp.mean(floats * floats, axis=-1, keepdims=True) + EPS)
    return (floats * inv_scale * gain_vec).astype(jnp.bfloat16)


def depthwise(gated_rows, conv_taps):
    span_width = conv_taps.shape[0]
    half_span = (span_width - 1) // 2
    seq_length = gated_rows.shape[1]
    padded = jnp.pad(
        gated_rows.astype(jnp.float32), ((0, 0), (half_span, span_width - 1 - half_span), (0, 0))
    )
    running = jnp.zeros(gated_rows.shape, jnp.float32)
    for tap_index in range(span_width):
        running = running + padded[:, tap_index : tap_index + seq_length] * conv_taps[
            tap_index
        ].astype(jnp.float32)
    return running


def passage_attention(queries, keys_values, head_count):
    groups, block_len, span_width = queries.shape
    head_dim = span_width // head_count
    row_count = keys_values.shape[1]
    query_heads = queries.reshape(groups, block_len, head_count, head_dim)
    key_heads = keys_values[:, :, :span_width].reshape(groups, row_count, head_count, head_dim)
    value_heads = keys_values[:, :, span_width:].reshape(groups, row_count, head_count, head_dim)
    scores = jnp.einsum(
        "gqhd,grhd->ghqr", query_heads, key_heads, preferred_element_type=jnp.float32
    ) * head_dim ** (-0.5)
    row_top = jnp.max(scores, axis=-1)
    exponent = jnp.exp(scores - row_top[..., None])
    row_sum = jnp.sum(exponent, axis=-1)
    weights = exponent.astype(jnp.bfloat16)
    outputs = jnp.einsum(
        "ghqr,grhd->gqhd", weights, value_heads, preferred_element_type=jnp.float32
    ).astype(jnp.bfloat16)
    return (outputs.reshape(groups, block_len, span_width), row_top, row_sum)


def combine(outs, tops, sums, head_count):
    batch_count, passage_count, block_len, span_width = outs.shape
    head_dim = span_width // head_count
    best_top = jnp.max(tops, axis=1, keepdims=True)
    weight = jnp.exp(tops - best_top)
    numerator = jnp.einsum(
        "bphq,bpqhd->bqhd",
        weight,
        outs.astype(jnp.float32).reshape(
            batch_count, passage_count, block_len, head_count, head_dim
        ),
    )
    denominator = jnp.sum(weight * sums, axis=1)
    result = numerator / jnp.transpose(denominator, (0, 2, 1))[..., None]
    return result.reshape(batch_count, block_len, span_width).astype(jnp.bfloat16)


def local(
    tokens,
    store,
    passage_ids,
    mix_gain,
    glu_value,
    glu_gate,
    conv_taps,
    channel_gain,
    mix_out,
    query_gain,
    passage_gain,
    query_proj,
    key_proj,
    value_proj,
    attn_out,
    blend_gain,
):
    owners = lax.axis_size("st")
    tok_rows = tokens.shape[0]
    model_width = tokens.shape[1]
    local_channels = glu_value.shape[1]
    head_width = query_proj.shape[1]
    local_heads = head_width // HD
    block_count = passage_ids.shape[0]
    per_block = passage_ids.shape[1]
    block_len = tok_rows // block_count
    requests = block_count * per_block
    capacity = 2 * requests // owners
    pass_local = store.shape[0]
    pass_rows = store.shape[1]
    flat_ids = passage_ids.reshape(requests)
    owner_of = flat_ids // pass_local
    local_of = flat_ids - owner_of * pass_local
    request_index = jnp.arange(requests)
    earlier = (owner_of[:, None] == owner_of[None, :]) & (
        request_index[None, :] < request_index[:, None]
    )
    ranking = jnp.sum(earlier.astype(jnp.int32), axis=1)
    slot_of = owner_of * capacity + ranking
    slot_ids = (
        jnp.zeros((owners * capacity,), jnp.int32)
        .at[slot_of]
        .set(local_of)
        .reshape(owners, capacity)
    )
    asked = lax.all_to_all(slot_ids, "st", split_axis=0, concat_axis=0, tiled=True)
    normed_store = rms_rows(store.reshape(pass_local * pass_rows, model_width), passage_gain)
    key_rows = jnp.dot(normed_store, key_proj, preferred_element_type=jnp.float32).astype(
        jnp.bfloat16
    )
    value_rows = jnp.dot(normed_store, value_proj, preferred_element_type=jnp.float32).astype(
        jnp.bfloat16
    )
    memory = jnp.concatenate([key_rows, value_rows], axis=1).reshape(
        pass_local, pass_rows, 2 * head_width
    )
    queries = jnp.dot(
        rms_rows(tokens, query_gain), query_proj, preferred_element_type=jnp.float32
    ).astype(jnp.bfloat16)
    query_blocks = queries.reshape(block_count, block_len, head_width)
    repeated = jnp.repeat(query_blocks, per_block, axis=0)
    served = memory[asked.reshape(owners * capacity)]
    slot_queries = (
        jnp.zeros((owners * capacity, block_len, head_width), jnp.bfloat16)
        .at[slot_of]
        .set(repeated)
    )
    visiting = lax.all_to_all(
        slot_queries.reshape(owners, capacity, block_len, head_width),
        "st",
        split_axis=0,
        concat_axis=0,
        tiled=True,
    )
    answer_out, answer_top, answer_sum = passage_attention(
        visiting.reshape(owners * capacity, block_len, head_width), served, local_heads
    )
    back_out = lax.all_to_all(
        answer_out.reshape(owners, capacity, block_len, head_width),
        "st",
        split_axis=0,
        concat_axis=0,
        tiled=True,
    )
    back_top, back_sum = (
        lax.all_to_all(
            answer_top.reshape(owners, capacity, local_heads, block_len),
            "st",
            split_axis=0,
            concat_axis=0,
            tiled=True,
        ),
        lax.all_to_all(
            answer_sum.reshape(owners, capacity, local_heads, block_len),
            "st",
            split_axis=0,
            concat_axis=0,
            tiled=True,
        ),
    )
    partial_out = back_out.reshape(owners * capacity, block_len, head_width)[slot_of]
    partial_top = back_top.reshape(owners * capacity, local_heads, block_len)[slot_of]
    partial_sum = back_sum.reshape(owners * capacity, local_heads, block_len)[slot_of]
    attended = combine(
        partial_out.reshape(block_count, per_block, block_len, head_width),
        partial_top.reshape(block_count, per_block, local_heads, block_len),
        partial_sum.reshape(block_count, per_block, local_heads, block_len),
        local_heads,
    ).reshape(tok_rows, head_width)
    mix_input = rms_rows(tokens, mix_gain)
    value_part = jnp.dot(mix_input, glu_value, preferred_element_type=jnp.float32)
    gate_part = jnp.dot(mix_input, glu_gate, preferred_element_type=jnp.float32)
    gated_rows = (value_part * jax.nn.sigmoid(gate_part)).astype(jnp.bfloat16)
    conv_rows = depthwise(gated_rows.reshape(-1, SEQ_LEN, local_channels), conv_taps).reshape(
        tok_rows, local_channels
    )
    channel_sum, channel_square = lax.psum(
        (jnp.sum(conv_rows, axis=1), jnp.sum(conv_rows * conv_rows, axis=1)), "tp"
    )
    row_mean = channel_sum / CA
    row_var = channel_square / CA - row_mean * row_mean
    activation = jax.nn.silu(
        (conv_rows - row_mean[:, None]) * lax.rsqrt(row_var + EPS)[:, None] * channel_gain
    ).astype(jnp.bfloat16)
    conv_term = jnp.dot(activation, mix_out, preferred_element_type=jnp.float32)
    attn_term = jnp.dot(attended, attn_out, preferred_element_type=jnp.float32)
    return lax.psum_scatter(
        (conv_term + blend_gain * attn_term).astype(jnp.bfloat16),
        "tp",
        scatter_dimension=0,
        tiled=True,
    )


def solution(mesh):
    in_specs = (
        P(("grp", "st"), None),
        P(("grp", "st"), None, None),
        P(("grp", "st"), None),
        P(),
        P(None, "tp"),
        P(None, "tp"),
        P(None, "tp"),
        P("tp"),
        P("tp", None),
        P(),
        P(),
        P(None, "tp"),
        P(None, "tp"),
        P(None, "tp"),
        P("tp", None),
        P(),
    )
    out_specs = P(("grp", "st", "tp"), None)
    return jax.shard_map(local, mesh=mesh, in_specs=in_specs, out_specs=out_specs, check_vma=False)
```

profile of v0, /device:TPU:0, one launch (start us, length us, event | category | flops | bytes accessed | tf_op | source)
XLA Modules:
  0.0 268.8 jit_solution(15184894235322269464)
XLA Ops:
  6.5 0.9 copy.39
  7.8 0.7 scatter_custom_fusion.1
  8.5 0.7 all_to_all.19
  9.2 4.3 %all-to-all-start.1 = ((s32[4,1,16]{2,1,0:T(1,128)}), s32[4,1,16]{2,1,0:T(1,128)S(1)}, u32[]{:S(2)}, u32[]{:S(2)}) async-start(s32[4,1,16]{2,1,0:T(1,128)} %bitcast.44), calls=%async_computation.1 | async-start | bytes 4096 | tf_op jit(solution)/shard_map/all_to_all | solution.py:118
  13.4 3.2 %multiply_reduce_fusion = f32[8,128]{1,0:T(8,128)S(1)} fusion(bf16[8,128,2048]{2,1,0:T(8,128)(2,1)} %param.17), kind=kLoop, calls=%fused_computation.9 | loop fusion | flops 6290432 | bytes 4198400 | tf_op jit(solution)/shard_map/reduce_sum | solution.py:16
  16.7 2.1 fusion.6
  18.8 2.9 %fusion.1 = bf16[1024,2048]{1,0:T(8,128)(2,1)} fusion(f32[2048]{0:T(1024)S(1)} %copy-done.8, f32[1024]{0:T(1024)S(1)} %rsqrt_bitcast_fusion, bf16[8,128,2048]{2,1,0:T(8,128)(2,1)S(1)} %copy-done.2), kind=kLoop, calls=%fused_computation.8 | loop fusion | flops 8388608 | bytes 8400896 | tf_op jit(solution)/shard_map/convert_element_type | solution.py:17
  21.8 1.3 fusion.20
  23.1 1.6 broadcast_in_dim.5
  24.7 2.5 broadcast_in_dim.4
  27.1 6.3 %scatter_fusion = bf16[64,64,512]{2,1,0:T(8,128)(2,1)} fusion(bf16[64,64,512]{2,1,0:T(8,128)(2,1)} %broadcast_in_dim.4, s32[32]{0:T(128)S(1)} %fusion.95, bf16[32,64,512]{2,1,0:T(8,128)(2,1)} %bitcast.117), kind=kCustom, calls=%fused_computation.4 | custom fusion | bytes 6291584 | tf_op jit(solution)/shard_map/scatter | solution.py:138
  33.4 5.0 %all-to-all-start = ((bf16[4,16,64,512]{3,2,1,0:T(8,128)(2,1)}), bf16[4,16,64,512]{3,2,1,0:T(8,128)(2,1)}, u32[]{:S(2)}, u32[]{:S(2)}) async-start(bf16[4,16,64,512]{3,2,1,0:T(8,128)(2,1)} %bitcast.116), calls=%async_computation | async-start | bytes 8388608 | tf_op jit(solution)/shard_map/all_to_all | solution.py:140
  38.5 5.4 %convolution_convert_fusion = bf16[1024,512]{0,1:T(8,128)(2,1)S(1)} fusion(bf16[1024,2048]{1,0:T(8,128)(2,1)} %fusion.1, bf16[2048,512]{1,0:T(8,128)(2,1)} %param.29), kind=kOutput, calls=%fused_computation.33 | convolution fusion | flops 2148007936 | bytes 7340032 | tf_op jit(solution)/shard_map/dot_general | solution.py:123
  43.9 2.4 convolution_convert_fusion.1
  46.3 1.5 pad_maximum_fusion
  47.8 4.0 %copy.55 = bf16[1024,1024]{1,0:T(8,128)(2,1)} copy(bf16[1024,1024]{0,1:T(8,128)(2,1)} %pad_maximum_fusion) | data formatting | bytes 4194304 | tf_op jit(solution)/shard_map/reshape | solution.py:126
  52.3 0.7 reduce.6
  53.0 8.9 %gather_fusion = bf16[64,128,1024]{2,1,0:T(8,128)(2,1)} fusion(bf16[8,128,1024]{2,1,0:T(8,128)(2,1)} %bitcast.113, s32[1024]{0:T(1024)S(1)} %pad_clamp_fusion.1), kind=kCustom, calls=%fused_computation | custom fusion | bytes 33554688 | tf_op jit(solution)/shard_map/gather | solution.py:134
  61.9 11.6 %fusion.102 = (bf16[64,128,512]{2,1,0:T(8,128)(2,1)}, bf16[64,128,512]{2,1,0:T(8,128)(2,1)}) fusion(bf16[64,128,1024]{2,1,0:T(8,128)(2,1)} %gather_fusion), kind=kLoop, calls=%fused_computation.202 | loop fusion | bytes 33554432 | tf_op jit(solution)/shard_map/slice | solution.py:41
  73.5 11.9 %copy.43 = bf16[64,128,512]{1,2,0:T(8,128)(2,1)} copy(bf16[64,128,512]{2,1,0:T(8,128)(2,1)} %get-tuple-element.13) | data formatting | bytes 16777216 | tf_op jit(solution)/shard_map/slice | solution.py:40
  85.4 11.9 %copy.46 = bf16[64,128,512]{1,2,0:T(8,128)(2,1)} copy(bf16[64,128,512]{2,1,0:T(8,128)(2,1)} %get-tuple-element.12) | data formatting | bytes 16777216 | tf_op jit(solution)/shard_map/slice | solution.py:41
  97.3 6.9 %reshape_reshape.6 = bf16[64,64,2,256]{3,2,1,0:T(2,128)(2,1)} reshape(bf16[4,16,64,512]{3,2,1,0:T(8,128)(2,1)} %all-to-all-done) | data formatting | bytes 8388608 | tf_op jit(solution)/shard_map/reshape;reshape | solution.py:39
  104.2 8.0 %multiply_reduce_fusion.1 = (f32[64,2,64]{2,1,0:T(2,128)S(1)}, f32[64,2,64,128]{3,2,1,0:T(8,128)}) fusion(bf16[64,128,2,256]{1,3,2,0:T(8,128)(2,1)} %bitcast.115, bf16[64,64,2,256]{3,2,1,0:T(2,128)(2,1)} %reshape_reshape.6), kind=kOutput, calls=%fused_computation.22 | convolution fusion | flops 538959872 | bytes 16809984 | tf_op jit(solution)/shard_map/gqhd,grhd->ghqr/dot_general | solution.py:42
  112.2 0.7 reshape.590
  112.9 3.3 %all-to-all-start.2 = ((f32[4,1,2048]{2,1,0:T(1,128)}), f32[4,1,2048]{2,1,0:T(1,128)S(1)}, u32[]{:S(2)}, u32[]{:S(2)}) async-start(f32[4,1,2048]{2,1,0:T(1,128)} %reshape.590), calls=%async_computation.2 | async-start | bytes 65536 | tf_op jit(solution)/shard_map/all_to_all | solution.py:158
  116.2 4.0 %fusion.9 = f32[64,2,64]{2,1,0:T(2,128)S(1)} fusion(f32[64,2,64,128]{3,2,1,0:T(8,128)} %get-tuple-element.48, f32[64,2,64]{2,1,0:T(2,128)S(1)} %get-tuple-element.47), kind=kLoop, calls=%fused_computation.23 | loop fusion | flops 3137536 | bytes 4259840 | tf_op jit(solution)/shard_map/reduce_sum | solution.py:47
  120.2 0.7 reshape.592
  120.9 3.5 %all-to-all-start.4 = ((f32[4,1,2048]{2,1,0:T(1,128)}), f32[4,1,2048]{2,1,0:T(1,128)S(1)}, u32[]{:S(2)}, u32[]{:S(2)}) async-start(f32[4,1,2048]{2,1,0:T(1,128)} %reshape.592), calls=%async_computation.4 | async-start | bytes 65536 | tf_op jit(solution)/shard_map/all_to_all | solution.py:165
  124.4 10.1 %convert_bitcast_fusion = bf16[64,64,2,256]{3,1,2,0:T(8,128)(2,1)S(1)} fusion(bf16[64,128,2,256]{1,3,2,0:T(8,128)(2,1)} %bitcast.114, f32[64,2,64,128]{3,2,1,0:T(8,128)} %get-tuple-element.48, f32[64,2,64]{2,1,0:T(2,128)S(1)} %get-tuple-element.47), kind=kOutput, calls=%fused_computation.20 | convolution fusion | flops 542113792 | bytes 16809984 | tf_op jit(solution)/shard_map/ghqr,grhd->gqhd/dot_general | solution.py:49
  134.5 6.3 %copy.48 = bf16[64,64,2,256]{3,2,1,0:T(2,128)(2,1)} copy(bf16[64,64,2,256]{3,1,2,0:T(8,128)(2,1)S(1)} %convert_bitcast_fusion) | data formatting | bytes 8388608 | tf_op jit(solution)/shard_map/convert_element_type | solution.py:51
  140.8 7.6 %reshape_reshape.7 = bf16[4,16,64,512]{3,2,1,0:T(8,128)(2,1)} reshape(bf16[64,64,2,256]{3,2,1,0:T(2,128)(2,1)} %copy.48) | data formatting | bytes 8388608 | tf_op jit(solution)/shard_map/reshape;reshape | solution.py:151
  148.5 5.1 %all-to-all-start.3 = ((bf16[4,16,64,512]{3,2,1,0:T(8,128)(2,1)}), bf16[4,16,64,512]{3,2,1,0:T(8,128)(2,1)}, u32[]{:S(2)}, u32[]{:S(2)}) async-start(bf16[4,16,64,512]{3,2,1,0:T(8,128)(2,1)} %reshape_reshape.7), calls=%async_computation.3 | async-start | bytes 8388608 | tf_op jit(solution)/shard_map/all_to_all | solution.py:150
  153.7 2.8 %fusion.25 = f32[512,256]{1,0:T(8,128)S(1)} fusion(bf16[2048,256]{1,0:T(8,128)(2,1)} %param.21, bf16[512,2048]{1,0:T(8,128)(2,1)} %param.16, f32[2048]{0:T(1024)S(1)} %copy-done.14, f32[512]{0:T(512)S(1)} %add_rsqrt_fusion.1), kind=kOutput, calls=%fused_computation.70 | convolution fusion | flops 541458432 | bytes 3680256 | tf_op jit(solution)/shard_map/dot_general | solution.py:184
  156.5 0.8 bitcast_convert_fusion
  157.3 2.4 fusion.100
  159.7 12.7 %all-reduce.1 = (f32[512]{0:T(512)S(1)}, f32[512]{0:T(512)S(1)}) all-reduce(f32[512]{0:T(512)S(1)} %bitcast.127, f32[512]{0:T(512)S(1)} %bitcast.126), channel_id=1, replica_groups=mesh['grp'=2,'st'=4,'tp'=4] {'tp'}, use_global_device_ids=true, to_apply=%region_4.5 | all-reduce | flops 1024 | bytes 8192 | tf_op jit(solution)/shard_map/psum | solution.py:189
  172.6 3.9 %fusion.103 = f32[512,2048]{1,0:T(8,128)} fusion(bf16[512,256]{1,0:T(8,128)(2,1)S(1)} %multiply_convert_fusion, bf16[256,2048]{1,0:T(8,128)(2,1)} %param.24), kind=kOutput, calls=%fused_computation.204 | convolution fusion | flops 536870912 | bytes 5505024 | tf_op jit(solution)/shard_map/dot_general | solution.py:197
  177.0 0.7 reduce.7
  177.8 0.6 gather_fusion.1
  178.9 0.7 reduce.8
  179.8 0.6 gather_fusion.3
  180.6 21.1 %all-to-all-done.3 = bf16[4,16,64,512]{3,2,1,0:T(8,128)(2,1)} async-done(((bf16[4,16,64,512]{3,2,1,0:T(8,128)(2,1)}), bf16[4,16,64,512]{3,2,1,0:T(8,128)(2,1)}, u32[]{:S(2)}, u32[]{:S(2)}) %all-to-all-start.3) | async-done | bytes 4194336 | tf_op jit(solution)/shard_map/all_to_all | solution.py:150
  201.7 4.2 %gather_fusion.2 = bf16[32,64,512]{2,1,0:T(8,128)(2,1)} fusion(bf16[64,64,512]{2,1,0:T(8,128)(2,1)} %bitcast.53, s32[1024]{0:T(1024)S(1)} %pad_clamp_fusion), kind=kCustom, calls=%fused_computation.2 | custom fusion | bytes 4194432 | tf_op jit(solution)/shard_map/gather | solution.py:173
  205.9 4.0 %reshape.492 = bf16[8,4,64,2,256]{4,3,2,1,0:T(2,128)(2,1)} reshape(bf16[32,64,512]{2,1,0:T(8,128)(2,1)} %gather_fusion.2) | data formatting | bytes 4194304 | tf_op jit(solution)/shard_map/reshape | solution.py:63
  209.9 3.7 %fusion.18 = f32[8,64,2,1,256]{4,3,2,1,0:T(1,128)S(1)} fusion(bf16[8,4,2,64,1]{1,4,2,3,0:T(2,128)(2,1)S(1)} %copy.52, bf16[8,4,64,2,256]{4,3,2,1,0:T(2,128)(2,1)} %reshape.492), kind=kOutput, calls=%fused_computation.31 | convolution fusion | flops 2097152 | bytes 3153920 | tf_op jit(solution)/shard_map/bphq,bpqhd->bqhd/dot_general | solution.py:60
  213.6 0.7 fusion.27
  214.5 2.7 %add_convert_fusion = bf16[512,2048]{1,0:T(8,128)(2,1)} fusion(f32[512,2048]{1,0:T(8,128)S(1)} %copy-done.1, bf16[512,512]{1,0:T(8,128)(2,1)S(1)} %bitcast.118, bf16[512,2048]{1,0:T(8,128)(2,1)S(1)} %copy-done, f32[2048]{0:T(1024)S(1)} %copy-done.7), kind=kOutput, calls=%fused_computation.19 | convolution fusion | flops 1076887552 | bytes 8921088 | tf_op jit(solution)/shard_map/dot_general | solution.py:198
  217.2 44.7 %reduce-scatter.2.cloned.1.call-done = bf16[128,2048]{1,0:T(8,128)(2,1)} async-done(((bf16[512,2048]{1,0:T(8,128)(2,1)}), bf16[128,2048]{1,0:T(8,128)(2,1)}) %reduce-scatter.2.cloned.1.call-update) | async-done | bytes 524304 | tf_op jit(solution)/shard_map/reduce_scatter | solution.py:199
  (61 shorter events, 2.9 us)
Async XLA Ops:
  6.5 207.9 %copy-start = (bf16[512,2048]{1,0:T(8,128)(2,1)S(1)}, bf16[512,2048]{1,0:T(8,128)(2,1)}, u32[]{:S(2)}) copy-start(bf16[512,2048]{1,0:T(8,128)(2,1)} %param.30) | copy-start | bytes 6291460
  6.5 12.2 %copy-start.8 = (f32[2048]{0:T(1024)S(1)}, f32[2048]{0:T(1024)}, u32[]{:S(2)}) copy-start(f32[2048]{0:T(1024)} %param.26) | copy-start | bytes 24580
  9.2 24.2 %all-to-all-start.1 = ((s32[4,1,16]{2,1,0:T(1,128)}), s32[4,1,16]{2,1,0:T(1,128)S(1)}, u32[]{:S(2)}, u32[]{:S(2)}) async-start(s32[4,1,16]{2,1,0:T(1,128)} %bitcast.44), calls=%async_computation.1 | async-start | bytes 4096 | tf_op jit(solution)/shard_map/all_to_all | solution.py:118
  13.4 5.3 %copy-start.2 = (bf16[8,128,2048]{2,1,0:T(8,128)(2,1)S(1)}, bf16[8,128,2048]{2,1,0:T(8,128)(2,1)}, u32[]{:S(2)}) copy-start(bf16[8,128,2048]{2,1,0:T(8,128)(2,1)} %param.17) | copy-start | bytes 12582916
  18.8 3.0 %copy-start.4 = (bf16[512,2048]{1,0:T(8,128)(2,1)S(1)}, bf16[512,2048]{1,0:T(8,128)(2,1)}, u32[]{:S(2)}) copy-start(bf16[512,2048]{1,0:T(8,128)(2,1)} %param.16) | copy-start | bytes 6291460
  18.8 3.0 %copy-start.10 = (bf16[2048,512]{1,0:T(8,128)(2,1)S(1)}, bf16[2048,512]{1,0:T(8,128)(2,1)}, u32[]{:S(2)}) copy-start(bf16[2048,512]{1,0:T(8,128)(2,1)} %param.27) | copy-start | bytes 6291460
  18.8 3.0 %copy-start.13 = (f32[2048]{0:T(1024)S(1)}, f32[2048]{0:T(1024)}, u32[]{:S(2)}) copy-start(f32[2048]{0:T(1024)} %param.25) | copy-start | bytes 24580
  33.4 63.9 %all-to-all-start = ((bf16[4,16,64,512]{3,2,1,0:T(8,128)(2,1)}), bf16[4,16,64,512]{3,2,1,0:T(8,128)(2,1)}, u32[]{:S(2)}, u32[]{:S(2)}) async-start(bf16[4,16,64,512]{3,2,1,0:T(8,128)(2,1)} %bitcast.116), calls=%async_computation | async-start | bytes 8388608 | tf_op jit(solution)/shard_map/all_to_all | solution.py:140
  38.5 5.4 %copy-start.3 = (bf16[1024,2048]{1,0:T(8,128)(2,1)S(1)}, bf16[1024,2048]{1,0:T(8,128)(2,1)}, u32[]{:S(2)}) copy-start(bf16[1024,2048]{1,0:T(8,128)(2,1)} %fusion.1) | copy-start | bytes 12582916
  38.5 5.4 %copy-start.11 = (bf16[2048,512]{1,0:T(8,128)(2,1)S(1)}, bf16[2048,512]{1,0:T(8,128)(2,1)}, u32[]{:S(2)}) copy-start(bf16[2048,512]{1,0:T(8,128)(2,1)} %param.28) | copy-start | bytes 6291460
  112.9 8.0 %all-to-all-start.2 = ((f32[4,1,2048]{2,1,0:T(1,128)}), f32[4,1,2048]{2,1,0:T(1,128)S(1)}, u32[]{:S(2)}, u32[]{:S(2)}) async-start(f32[4,1,2048]{2,1,0:T(1,128)} %reshape.590), calls=%async_computation.2 | async-start | bytes 65536 | tf_op jit(solution)/shard_map/all_to_all | solution.py:158
  120.9 27.5 %all-to-all-start.4 = ((f32[4,1,2048]{2,1,0:T(1,128)}), f32[4,1,2048]{2,1,0:T(1,128)S(1)}, u32[]{:S(2)}, u32[]{:S(2)}) async-start(f32[4,1,2048]{2,1,0:T(1,128)} %reshape.592), calls=%async_computation.4 | async-start | bytes 65536 | tf_op jit(solution)/shard_map/all_to_all | solution.py:165
  148.4 5.1 %copy-start.6 = (bf16[31,256]{1,0:T(8,128)(2,1)S(1)}, bf16[31,256]{1,0:T(8,128)(2,1)}, u32[]{:S(2)}) copy-start(bf16[31,256]{1,0:T(8,128)(2,1)} %param.22) | copy-start | bytes 47620
  148.4 5.2 %copy-start.14 = (f32[2048]{0:T(1024)S(1)}, f32[2048]{0:T(1024)}, u32[]{:S(2)}) copy-start(f32[2048]{0:T(1024)} %param.19) | copy-start | bytes 24580
  148.5 53.3 %all-to-all-start.3 = ((bf16[4,16,64,512]{3,2,1,0:T(8,128)(2,1)}), bf16[4,16,64,512]{3,2,1,0:T(8,128)(2,1)}, u32[]{:S(2)}, u32[]{:S(2)}) async-start(bf16[4,16,64,512]{3,2,1,0:T(8,128)(2,1)} %reshape_reshape.7), calls=%async_computation.3 | async-start | bytes 8388608 | tf_op jit(solution)/shard_map/all_to_all | solution.py:150
  153.5 108.4 %reduce-scatter.2.cloned.1.call-start = ((), (), s32[]{:S(2)}) async-start(), calls=%async_computation.6 | async-start | bytes 2621440 | tf_op jit(solution)/shard_map/reduce_scatter | solution.py:199
  153.6 2.9 %copy-start.5 = (bf16[512,2048]{1,0:T(8,128)(2,1)S(1)}, bf16[512,2048]{1,0:T(8,128)(2,1)}, u32[]{:S(2)}) copy-start(bf16[512,2048]{1,0:T(8,128)(2,1)} %param.16) | copy-start | bytes 6291460
  153.6 2.9 %copy-start.12 = (bf16[2048,256]{1,0:T(8,128)(2,1)S(1)}, bf16[2048,256]{1,0:T(8,128)(2,1)}, u32[]{:S(2)}) copy-start(bf16[2048,256]{1,0:T(8,128)(2,1)} %param.20) | copy-start | bytes 3145732
  156.5 15.9 %copy-start.9 = (f32[256]{0:T(256)S(1)}, f32[256]{0:T(256)}, u32[]{:S(2)}) copy-start(f32[256]{0:T(256)} %param.23) | copy-start | bytes 3076
  209.9 4.5 %copy-start.1 = (f32[512,2048]{1,0:T(8,128)S(1)}, f32[512,2048]{1,0:T(8,128)}, u32[]{:S(2)}) copy-start(f32[512,2048]{1,0:T(8,128)} %fusion.103) | copy-start | bytes 12582916
  209.9 4.6 %copy-start.7 = (f32[2048]{0:T(1024)S(1)}, f32[2048]{0:T(1024)}, u32[]{:S(2)}) copy-start(f32[2048]{0:T(1024)} %param.31) | copy-start | bytes 24580
Sparse Core Ops, SparseCore 0:
  217.3 44.5 reduce-scatter.1
where the time goes:
time: 270 us; the launch traced here: 269 us
  local copies, waits for them, and re-layouts  94.7 us (35%)
  waiting for transfers between devices  65.9 us (24%)
  matrix products  41 us (15%)
  starting transfers between devices  21.2 us (8%)
  other arithmetic  19.6 us (7%)
  between operations  13.8 us (5%)
  blocking collectives  12.7 us (5%)
    reduce_scatter x1, waiting for transfers between devices, local(): lax.psum_scatter((conv_term + blend_gain * attn_term).astype(jnp.bfloat16...  44.7 us
    slice x2, local copies, waits for them, and re-layouts, passage_attention(): keys_values[:, :, span_width:]  23.5 us
    all_to_all x1, waiting for transfers between devices, local(): lax.all_to_all(answer_out.reshape(owners, capacity, block_len, head_width...  21.1 us
    psum x1, blocking collectives, local(): lax.psum((jnp.sum(conv_rows, axis=1), jnp.sum(conv_rows * conv_rows, axis...  12.7 us
    slice x1, local copies, waits for them, and re-layouts, passage_attention(): keys_values[:, :, :span_width]  11.9 us
    dot_general x1, matrix products, passage_attention(): jnp.einsum('ghqr,grhd->gqhd', weights, value_heads, preferred_element_typ...  10.1 us
    gather x1, local copies, waits for them, and re-layouts, local(): served = memory[asked.reshape(owners * capacity)]  8.92 us
    dot_general x1, matrix products, passage_attention(): jnp.einsum('gqhd,grhd->ghqr', query_heads, key_heads, preferred_element_t...  7.98 us
  transfers between devices with their start and end apart: 6, of which 2 were waited for; matrix products, arithmetic and copies ran while one was open for 45% of the time, Pallas kernels for 0%

commit v1 on v0

--- a/solution.py
+++ b/solution.py
@@ -1,7 +1,11 @@
+import functools
+
 import jax
 import jax.numpy as jnp
 from jax import lax
 from jax.sharding import PartitionSpec as P
+from jax.experimental import pallas as pl
+from jax.experimental.pallas import tpu as pltpu
 
 CA = 1024
 HD = 256
@@ -204,6 +208,417 @@
     )
 
 
+BF = jnp.bfloat16
+F32 = jnp.float32
+NEG = -3e38
+
+
+def mm(a, b):
+    return jnp.dot(a, b, preferred_element_type=F32)
+
+
+def wait_in(ref, sem):
+    pltpu.make_async_copy(ref, ref, sem).wait()
+
+
+def layer_kernel(
+    n_st, n_tp, block_count, per_block, block_len, local_heads, seq_len, pass_rows,
+    tokens_h, store_h, ids_v, mix_gain, gv_h, gg_h, taps, channel_gain, mo_h, query_gain,
+    passage_gain, qw_h, kw_h, vw_h, ao_h, blend_gain,
+    out_ref,
+    tok, sto, gv, gg, mo, qw, kw, vw, ao, load_sem,
+    ids_all, ids_s, ids_send, ids_recv, ids_sem,
+    q_all, q_stage, q_send, q_recv,
+    k_all, v_all, k_stage, v_stage, kv_send, kv_recv,
+    gp, conv, scol, stat_all, stat_send, stat_recv, act,
+    out_o, out_s, ret_o, ret_s, o_send, o_recv, s_send, s_recv, att,
+    part, from_left, from_right, r_send, r_recv,
+):
+    st = lax.axis_index("st")
+    tp = lax.axis_index("tp")
+    core = lax.rem(st, 2)
+    chip = st // 2
+    n_chip = n_st // 2
+    other = 1 - core
+    T = tok.shape[0]
+    R = sto.shape[0]
+    HW = q_stage.shape[1]
+    CL = act.shape[1]
+
+    loads = []
+    for n, (a, b) in enumerate(
+        [(tokens_h, tok), (qw_h, qw), (gv_h, gv), (gg_h, gg), (store_h, sto), (kw_h, kw),
+         (vw_h, vw), (mo_h, mo), (ao_h, ao)]
+    ):
+        c = pltpu.make_async_copy(a, b, load_sem.at[n])
+        c.start()
+        loads.append(c)
+
+    barrier = pltpu.get_barrier_semaphore()
+    for i in range(1, n_st):
+        pl.semaphore_signal(barrier, inc=1, device_id={"st": lax.rem(st + i, n_st)},
+                            device_id_type=pl.DeviceIdType.MESH)
+    for i in range(1, n_tp):
+        pl.semaphore_signal(barrier, inc=1, device_id={"tp": lax.rem(tp + i, n_tp)},
+                            device_id_type=pl.DeviceIdType.MESH)
+
+    def remote(src, dst, ssem, rsem, axis, to):
+        return pltpu.make_async_remote_copy(
+            src_ref=src, dst_ref=dst, send_sem=ssem, recv_sem=rsem, device_id={axis: to},
+            device_id_type=pl.DeviceIdType.MESH)
+
+    pl.semaphore_wait(barrier, n_st - 1 + n_tp - 1)
+
+    for i in range(1, n_st):
+        remote(ids_v, ids_all.at[st], ids_send.at[i], ids_recv.at[st], "st",
+               lax.rem(st + i, n_st)).start()
+    ids_own = pltpu.make_async_copy(ids_v, ids_all.at[st], ids_recv.at[st])
+    ids_own.start()
+
+    for n in range(4):
+        loads[n].wait()
+    TC = 256
+    n_tc = T // TC
+    per_seq = seq_len
+    pad = (gp.shape[1] - per_seq) // 2
+    gp[:, :pad] = jnp.zeros((gp.shape[0], pad, CL), F32)
+    gp[:, pad + per_seq:] = jnp.zeros((gp.shape[0], pad, CL), F32)
+
+    def peers():
+        res = [(chip * 2 + other, True, 0)]
+        for j in range(1, n_chip):
+            c = lax.rem(chip + j, n_chip)
+            res.append((c * 2 + core, False, 2 * j - 1))
+            res.append((c * 2 + other, True, 2 * j))
+        return res
+
+    def tok_chunk(i, carry):
+        rows = pl.ds(pl.multiple_of(i * TC, TC), TC)
+        x = tok[rows, :].astype(F32)
+        y = x * lax.rsqrt(jnp.mean(x * x, axis=-1, keepdims=True) + EPS)
+        qr = (y * query_gain[...]).astype(BF)
+        q_all[st, rows, :] = mm(qr, qw[:, pl.ds(pl.multiple_of(core * HW, HW), HW)]).astype(BF)
+        q_stage[rows, :] = mm(qr, qw[:, pl.ds(pl.multiple_of(other * HW, HW), HW)]).astype(BF)
+        for to, stage, n in peers():
+            src = q_stage.at[rows] if stage else q_all.at[st, rows]
+            remote(src, q_all.at[st, rows], q_send.at[n, i], q_recv.at[st, i], "st", to).start()
+        mr = (y * mix_gain[...]).astype(BF)
+        gated = (mm(mr, gv[...]) * jax.nn.sigmoid(mm(mr, gg[...]))).astype(BF).astype(F32)
+        for u in range(TC // per_seq):
+            gp[i * (TC // per_seq) + u, pad:pad + per_seq, :] = gated[u * per_seq:(u + 1) * per_seq]
+        return carry
+
+    lax.fori_loop(0, n_tc, tok_chunk, 0)
+
+    for n in range(4, 7):
+        loads[n].wait()
+    RC = 256
+    n_rc = R // RC
+    RP = RC // pass_rows
+    pass_local = R // pass_rows
+    mine = pl.ds(pl.multiple_of(core * HW, HW), HW)
+    theirs = pl.ds(pl.multiple_of(other * HW, HW), HW)
+    partner = chip * 2 + other
+
+    def store_chunk(i, carry):
+        rows = pl.ds(pl.multiple_of(i * RC, RC), RC)
+        x = sto[rows, :].astype(F32)
+        n = (x * lax.rsqrt(jnp.mean(x * x, axis=-1, keepdims=True) + EPS) * passage_gain[...]).astype(BF)
+        here, slots = pl.ds(i * RP, RP), pl.ds(core * pass_local + i * RP, RP)
+        k_stage[here] = mm(n, kw[:, theirs]).astype(BF).reshape(RP, pass_rows, HW)
+        v_stage[here] = mm(n, vw[:, theirs]).astype(BF).reshape(RP, pass_rows, HW)
+        remote(k_stage.at[here], k_all.at[slots], kv_send.at[0, i], kv_recv.at[0, i], "st", partner).start()
+        remote(v_stage.at[here], v_all.at[slots], kv_send.at[1, i], kv_recv.at[1, i], "st", partner).start()
+        k_all[slots] = mm(n, kw[:, mine]).astype(BF).reshape(RP, pass_rows, HW)
+        v_all[slots] = mm(n, vw[:, mine]).astype(BF).reshape(RP, pass_rows, HW)
+        return carry
+
+    lax.fori_loop(0, n_rc, store_chunk, 0)
+
+    tap_values = taps[...].astype(F32)
+    n_tap = taps.shape[0]
+    lead = pad - (n_tap - 1) // 2
+    CC = 32
+    per = per_seq // CC
+    lane = lax.broadcasted_iota(jnp.int32, (CC, 128), 1)
+
+    def conv_chunk(i, carry):
+        seq = i // per
+        base = pl.multiple_of(lax.rem(i, per) * CC, CC)
+        win = gp[seq, pl.ds(base, CC + 2 * pad), :]
+        acc = jnp.zeros((CC, CL), F32)
+        for k in range(n_tap):
+            acc = acc + win[lead + k:lead + k + CC] * tap_values[k:k + 1]
+        rows = pl.ds(pl.multiple_of(i * CC, CC), CC)
+        conv[rows, :] = acc
+        s = jnp.sum(acc, axis=1, keepdims=True)
+        ss = jnp.sum(acc * acc, axis=1, keepdims=True)
+        scol[rows, :] = jnp.where(lane == 0, s, jnp.where(lane == 1, ss, 0.0))
+        return carry
+
+    lax.fori_loop(0, T // CC, conv_chunk, 0)
+    stat_all[tp] = jnp.transpose(scol[...])[:8]
+    for i in range(1, n_tp):
+        remote(stat_all.at[tp], stat_all.at[tp], stat_send.at[i], stat_recv.at[tp], "tp",
+               lax.rem(tp + i, n_tp)).start()
+
+    ids_own.wait()
+    for i in range(1, n_st):
+        r = lax.rem(st + i, n_st)
+        remote(ids_v, ids_all.at[r], ids_send.at[i], ids_recv.at[r], "st", r).wait_recv()
+    c = pltpu.make_async_copy(ids_all, ids_s, ids_sem)
+    c.start()
+    c.wait()
+
+    def kv_wait(i, carry):
+        here, slots = pl.ds(i * RP, RP), pl.ds(other * pass_local + i * RP, RP)
+        remote(k_stage.at[here], k_all.at[slots], kv_send.at[0, i], kv_recv.at[0, i], "st", partner).wait()
+        remote(v_stage.at[here], v_all.at[slots], kv_send.at[1, i], kv_recv.at[1, i], "st", partner).wait()
+        return carry
+
+    lax.fori_loop(0, n_rc, kv_wait, 0)
+
+    heads = local_heads // 2
+    HD_ = HW // heads
+    per_chip = 2 * pass_local
+    blane = lax.broadcasted_iota(jnp.int32, (block_len, 128), 1)
+    scale = HD_ ** (-0.5)
+
+    def order(i):
+        return lax.rem(chip + 1 + i // 2, n_chip) * 2 + lax.rem(core + 1 - i % 2, 2)
+
+    for i in range(n_st):
+        r = order(i)
+        own = i == n_st - 1
+        if not own:
+            def q_wait(j, carry, r=r):
+                rows = pl.ds(pl.multiple_of(j * TC, TC), TC)
+                remote(q_all.at[st, rows], q_all.at[r, rows], q_send.at[0, j], q_recv.at[r, j], "st", r).wait_recv()
+                return carry
+            lax.fori_loop(0, n_tc, q_wait, 0)
+
+        def block(b, carry, r=r, own=own):
+            rows = pl.ds(pl.multiple_of(b * block_len, block_len), block_len)
+            stats = jnp.zeros((block_len, 128), F32)
+            for h in range(heads):
+                cols = slice(h * HD_, (h + 1) * HD_)
+                q = q_all[r, rows, cols]
+                tops, sums, outs, valids = [], [], [], []
+                for j in range(per_block):
+                    p = ids_s[r, b, j] - chip * per_chip
+                    spread_p = jnp.full((block_len, 1), p, jnp.int32)
+                    valid = jnp.logical_and(spread_p >= 0, spread_p < per_chip)
+                    slot = jnp.clip(p, 0, per_chip - 1)
+                    k = k_all[slot][:, cols]
+                    v = v_all[slot][:, cols]
+                    s = lax.dot_general(q, k, (((1,), (1,)), ((), ())), preferred_element_type=F32) * scale
+                    top = jnp.max(s, axis=1, keepdims=True)
+                    e = jnp.exp(s - top)
+                    sums.append(jnp.sum(e, axis=1, keepdims=True))
+                    outs.append(mm(e.astype(BF), v).astype(BF).astype(F32))
+                    tops.append(jnp.where(valid, top, NEG))
+                    valids.append(valid)
+                best = functools.reduce(jnp.maximum, tops)
+                num, den = 0.0, 0.0
+                for j in range(per_block):
+                    w = jnp.where(valids[j], jnp.exp(tops[j] - best), 0.0)
+                    num = num + w * outs[j]
+                    den = den + w * sums[j]
+                if own:
+                    ret_o[st, rows, cols] = num.astype(BF)
+                else:
+                    out_o[r, rows, cols] = num.astype(BF)
+                stats = jnp.where(blane == 2 * h, best, jnp.where(blane == 2 * h + 1, den, stats))
+            scol[rows, :] = stats
+            return carry
+
+        lax.fori_loop(0, block_count, block, 0)
+        packed = jnp.transpose(scol[...])[:8]
+        if own:
+            ret_s[st] = packed
+        else:
+            out_s[r] = packed
+            remote(out_o.at[r], ret_o.at[st], o_send.at[r], o_recv.at[st], "st", r).start()
+            remote(out_s.at[r], ret_s.at[st], s_send.at[r], s_recv.at[st], "st", r).start()
+
+    total = stat_all[tp]
+    for i in range(1, n_tp):
+        r = lax.rem(tp + i, n_tp)
+        remote(stat_all.at[tp], stat_all.at[r], stat_send.at[i], stat_recv.at[r], "tp", r).wait_recv()
+        total = total + stat_all[r]
+    ca = CL * n_tp
+    mean = total / ca
+    spread = jnp.transpose(jnp.concatenate([mean, jnp.zeros((120, T), F32)], axis=0))
+    row_mean = spread[:, 0:1]
+    inv = lax.rsqrt(spread[:, 1:2] - row_mean * row_mean + EPS)
+    a = (conv[...] - row_mean) * inv * channel_gain[...]
+    act[...] = (a / (1.0 + jnp.exp(-a))).astype(BF)
+
+    for i in range(n_st - 1):
+        r = order(i)
+        remote(out_o.at[r], ret_o.at[r], o_send.at[r], o_recv.at[r], "st", r).wait_recv()
+        remote(out_s.at[r], ret_s.at[r], s_send.at[r], s_recv.at[r], "st", r).wait_recv()
+    for g in range(2):
+        cols_of = [jnp.transpose(jnp.concatenate([ret_s[c * 2 + g], jnp.zeros((120, T), F32)], axis=0))
+                   for c in range(n_chip)]
+        for h in range(heads):
+            cols = slice(h * HD_, (h + 1) * HD_)
+            best = functools.reduce(jnp.maximum, [x[:, 2 * h:2 * h + 1] for x in cols_of])
+            num, den = 0.0, 0.0
+            for c in range(n_chip):
+                w = jnp.exp(cols_of[c][:, 2 * h:2 * h + 1] - best)
+                num = num + w * ret_o[c * 2 + g, :, cols].astype(F32)
+                den = den + w * cols_of[c][:, 2 * h + 1:2 * h + 2]
+            att[:, g * HW + h * HD_:g * HW + (h + 1) * HD_] = (num / den).astype(BF)
+
+    loads[7].wait()
+    loads[8].wait()
+    NC = 512
+    n_nc = part.shape[1] // NC
+
+    def out_cols(i, carry):
+        cols = pl.ds(pl.multiple_of(i * NC, NC), NC)
+        value = mm(act[...], mo[:, cols]) + blend_gain[:, cols] * mm(att[...], ao[:, cols])
+        part[:, cols] = value.astype(BF)
+        return carry
+
+    lax.fori_loop(0, n_nc, out_cols, 0)
+
+    rows_out = out_ref.shape[0]
+    SUB = 4
+    SR = rows_out // SUB
+
+    def hop(d, u, ahead, buf, way, go, first, last):
+        prow = pl.ds(pl.multiple_of(d * rows_out + u * SR, SR), SR)
+        brow = pl.ds(u * SR, SR)
+        to = jnp.clip(tp + ahead, 0, n_tp - 1)
+        copy = remote(part.at[prow], buf.at[d, brow], r_send.at[way, d, u], r_recv.at[way, d, u], "tp", to)
+
+        @pl.when(jnp.logical_and(go, jnp.logical_not(first)))
+        def _():
+            copy.wait_recv()
+            part[prow, :] = (part[prow, :].astype(F32) + buf[d, brow, :].astype(F32)).astype(BF)
+
+        @pl.when(go)
+        def _():
+            copy.start()
+
+    for i in range(1, n_tp):
+        for u in range(SUB):
+            d = n_tp - i
+            hop(d, u, 1, from_left, 0, tp < d, tp == 0, None)
+            d = i - 1
+            hop(d, u, -1, from_right, 1, tp > d, tp == n_tp - 1, None)
+
+    for u in range(SUB):
+        prow = pl.ds(pl.multiple_of(tp * rows_out + u * SR, SR), SR)
+        brow = pl.ds(u * SR, SR)
+        out_acc = part[prow, :].astype(F32)
+        conv_rows = brow
+
+        @pl.when(tp > 0)
+        def _():
+            remote(part.at[prow], from_left.at[tp, brow], r_send.at[0, tp, u], r_recv.at[0, tp, u], "tp",
+                   jnp.maximum(tp - 1, 0)).wait_recv()
+
+        @pl.when(tp == 0)
+        def _():
+            from_left[0, brow, :] = jnp.zeros((SR, part.shape[1]), BF)
+
+        @pl.when(tp < n_tp - 1)
+        def _():
+            remote(part.at[prow], from_right.at[tp, brow], r_send.at[1, tp, u], r_recv.at[1, tp, u], "tp",
+                   jnp.minimum(tp + 1, n_tp - 1)).wait_recv()
+
+        @pl.when(tp == n_tp - 1)
+        def _():
+            from_right[n_tp - 1, brow, :] = jnp.zeros((SR, part.shape[1]), BF)
+
+        out_ref[brow, :] = (
+            out_acc + from_left[tp, brow, :].astype(F32) + from_right[tp, brow, :].astype(F32)
+        ).astype(BF)
+
+    for i in range(1, n_st):
+        r = lax.rem(st + i, n_st)
+        remote(ids_v, ids_all.at[st], ids_send.at[i], ids_recv.at[st], "st", r).wait_send()
+    for i in range(n_tc):
+        rows = pl.ds(i * TC, TC)
+        for to, stage, n in peers():
+            src = q_stage.at[rows] if stage else q_all.at[st, rows]
+            remote(src, q_all.at[st, rows], q_send.at[n, i], q_recv.at[st, i], "st", to).wait_send()
+    for i in range(1, n_tp):
+        remote(stat_all.at[tp], stat_all.at[tp], stat_send.at[i], stat_recv.at[tp], "tp",
+               lax.rem(tp + i, n_tp)).wait_send()
+    for i in range(n_st - 1):
+        r = order(i)
+        remote(out_o.at[r], ret_o.at[st], o_send.at[r], o_recv.at[st], "st", r).wait_send()
+        remote(out_s.at[r], ret_s.at[st], s_send.at[r], s_recv.at[st], "st", r).wait_send()
+    for d in range(n_tp):
+        for u in range(SUB):
+            prow = pl.ds(d * rows_out + u * SR, SR)
+
+            @pl.when(tp < d)
+            def _():
+                remote(part.at[prow], from_left.at[d, pl.ds(u * SR, SR)], r_send.at[0, d, u],
+                       r_recv.at[0, d, u], "tp", jnp.minimum(tp + 1, n_tp - 1)).wait_send()
+
+            @pl.when(tp > d)
+            def _():
+                remote(part.at[prow], from_right.at[d, pl.ds(u * SR, SR)], r_send.at[1, d, u],
+                       r_recv.at[1, d, u], "tp", jnp.maximum(tp - 1, 0)).wait_send()
+
+
+def fused_local(
+    tokens, store, passage_ids, mix_gain, glu_value, glu_gate, conv_taps, channel_gain, mix_out,
+    query_gain, passage_gain, query_proj, key_proj, value_proj, attn_out, blend_gain,
+):
+    n_st = lax.axis_size("st")
+    n_tp = lax.axis_size("tp")
+    T, D = tokens.shape
+    P_, PR, _ = store.shape
+    R = P_ * PR
+    W = query_proj.shape[1]
+    HW = W // 2
+    CL = glu_value.shape[1]
+    nb, per_block = passage_ids.shape
+    ids = jnp.pad(passage_ids, ((0, 0), (0, 128 - per_block)))
+    pad = 8 * pl.cdiv((conv_taps.shape[0] - 1) // 2, 8)
+    DMA = pltpu.SemaphoreType.DMA
+    V = pltpu.VMEM
+    SUB = 4
+    kern = functools.partial(layer_kernel, n_st, n_tp, nb, per_block, T // nb, W // HD, SEQ_LEN, PR)
+    hbm = pl.BlockSpec(memory_space=pl.ANY)
+    vm = pl.BlockSpec(memory_space=pltpu.VMEM)
+    return pl.pallas_call(
+        kern,
+        out_shape=jax.ShapeDtypeStruct((T // n_tp, D), BF),
+        in_specs=[hbm, hbm, vm, vm, hbm, hbm, vm, vm, hbm, vm, vm, hbm, hbm, hbm, hbm, vm],
+        out_specs=vm,
+        scratch_shapes=[
+            V((T, D), BF), V((R, D), BF), V((D, CL), BF), V((D, CL), BF), V((CL, D), BF),
+            V((D, W), BF), V((D, W), BF), V((D, W), BF), V((W, D), BF), DMA((9,)),
+            V((n_st, nb, 128), jnp.int32), pltpu.SMEM((n_st, nb, 128), jnp.int32),
+            DMA((n_st,)), DMA((n_st,)), DMA,
+            V((n_st, T, HW), BF), V((T, HW), BF), DMA((n_st - 1, T // 256)), DMA((n_st, T // 256)),
+            V((2 * P_, PR, HW), BF), V((2 * P_, PR, HW), BF), V((P_, PR, HW), BF), V((P_, PR, HW), BF),
+            DMA((2, R // 256)), DMA((2, R // 256)),
+            V((T // SEQ_LEN, SEQ_LEN + 2 * pad, CL), F32), V((T, CL), F32), V((T, 128), F32),
+            V((n_tp, 8, T), F32), DMA((n_tp,)), DMA((n_tp,)), V((T, CL), BF),
+            V((n_st, T, HW), BF), V((n_st, 8, T), F32), V((n_st, T, HW), BF), V((n_st, 8, T), F32),
+            DMA((n_st,)), DMA((n_st,)), DMA((n_st,)), DMA((n_st,)), V((T, W), BF),
+            V((T, D), BF), V((n_tp, T // n_tp, D), BF), V((n_tp, T // n_tp, D), BF),
+            DMA((2, n_tp, SUB)), DMA((2, n_tp, SUB)),
+        ],
+        compiler_params=pltpu.CompilerParams(
+            collective_id=0, has_side_effects=True, vmem_limit_bytes=60 * 1024 * 1024),
+        name="layer",
+    )(
+        tokens, store.reshape(R, D), ids, mix_gain.reshape(1, D), glu_value, glu_gate, conv_taps,
+        channel_gain.reshape(1, CL), mix_out, query_gain.reshape(1, D), passage_gain.reshape(1, D),
+        query_proj, key_proj, value_proj, attn_out, blend_gain.reshape(1, D),
+    )
+
+
 def solution(mesh):
     in_specs = (
         P(("grp", "st"), None),
@@ -224,4 +639,8 @@
         P(),
     )
     out_specs = P(("grp", "st", "tp"), None)
-    return jax.shard_map(local, mesh=mesh, in_specs=in_specs, out_specs=out_specs, check_vma=False)
+    def body(*args):
+        even = args[11].shape[1] // HD % 2 == 0 and mesh.shape["st"] % 2 == 0
+        return (fused_local if even else local)(*args)
+
+    return jax.shard_map(body, mesh=mesh, in_specs=in_specs, out_specs=out_specs, check_vma=False)

time: 270 us -> 110 us (0.41)
  Pallas kernels: 0 us -> 105 us
  local copies, waits for them, and re-layouts: 94.7 us -> 3.24 us
  waiting for transfers between devices: 65.9 us -> 0 us
  matrix products: 41 us -> 0 us
  starting transfers between devices: 21.2 us -> 0 us
  other arithmetic: 19.6 us -> 0 us
  between operations: 13.8 us -> 0.01 us
  blocking collectives: 12.7 us -> 0 us
    pallas_call x0 -> x1, Pallas kernels: none -> 105 us  [fused_local(): pl.pallas_call(kern, out_shape=jax.ShapeDtypeStruct((T // n_tp, D), BF),...]
    reduce_scatter x1 -> x0, waiting for transfers between devices: 44.7 us -> none  [local(): lax.psum_scatter((conv_term + blend_gain * attn_term).astype(jnp.bfloat16...]
    dot_general x10 -> x0, matrix products: 41 us -> none  [the longest x1 10.1 us: passage_attention(): jnp.einsum('ghqr,grhd->gqhd', weights, value_heads, preferred_element_typ...]
    slice x3 -> x0, local copies, waits for them, and re-layouts: 35.3 us -> none  [the longest x2 23.5 us: passage_attention(): keys_values[:, :, span_width:]]
    all_to_all x5 -> x0, waiting for transfers between devices: 21.1 us -> none  [the longest x1 21.1 us: local(): lax.all_to_all(answer_out.reshape(owners, capacity, block_len, head_width...]
    all_to_all x5 -> x0, starting transfers between devices: 21.1 us -> none  [the longest x1 5.08 us: local(): lax.all_to_all(answer_out.reshape(owners, capacity, block_len, head_width...]
    another operation x2 -> x0, local copies, waits for them, and re-layouts: 14.5 us -> none  [the longest x1 7.6 us: local(): answer_out.reshape(owners, capacity, block_len, head_width)]
    gather x4 -> x0, local copies, waits for them, and re-layouts: 14.3 us -> none  [the longest x1 8.92 us: local(): served = memory[asked.reshape(owners * capacity)]]
  transfers between devices with their start and end apart: 6 -> 0, of which waited for: 2 -> 0; matrix products, arithmetic and copies ran while one was open for 45% -> 0% of each run, Pallas kernels for 0% -> 0%
where the time goes in v1:
time: 110 us; the launch traced here: 108 us
  Pallas kernels  105 us (95%)
  local copies, waits for them, and re-layouts  3.24 us (3%)
    pallas_call x1, Pallas kernels, fused_local(): pl.pallas_call(kern, out_shape=jax.ShapeDtypeStruct((T // n_tp, D), BF),...  105 us
    unnamed x2, local copies, waits for them, and re-layouts  2.64 us

profile of v1, /device:TPU:0, one launch (start us, length us, event | category | flops | bytes accessed | tf_op | source)
XLA Modules:
  0.0 108.2 jit_solution(18147269409609720201)
XLA Ops:
  0.0 0.8 copy.17
  0.8 0.6 pad.4.ids_v
  1.4 104.9 %layer.1 = bf16[128,2048]{1,0:T(8,128)(2,1)} custom-call(bf16[512,2048]{1,0:T(8,128)(2,1)} %tokens_h.1, bf16[1024,2048]{1,0:T(8,128)(2,1)} %bitcast.6, s32[8,128]{1,0:T(8,128)} %pad.4.ids_v, f32[1,2048]{1,0:T(1,128)} %bitcast.7, bf16[2048,256]{1,0:T(8,128)(2,1)} %gv_h.1, bf16[2048,256]{1,0:T(8,128)(2,1)} %gg_h.1, bf16[31,256]{1,0:T(8,128)(2,1)} %taps.1, ...), custom_call_target="tpu_custom_call" | custom-call | tf_op jit(solution)/shard_map/layer/pallas_call | solution.py:592
  106.3 1.9 %copy.19 = bf16[128,2048]{1,0:T(8,128)(2,1)} copy(bf16[128,2048]{1,0:T(8,128)(2,1)} %layer.1) | data formatting | bytes 1048576

commit v2 on v0

--- a/solution.py
+++ b/solution.py
@@ -1,7 +1,11 @@
+import functools
+
 import jax
 import jax.numpy as jnp
 from jax import lax
 from jax.sharding import PartitionSpec as P
+from jax.experimental import pallas as pl
+from jax.experimental.pallas import tpu as pltpu
 
 CA = 1024
 HD = 256
@@ -204,6 +208,456 @@
     )
 
 
+BF = jnp.bfloat16
+F32 = jnp.float32
+NEG = -3e38
+
+
+def mm(a, b):
+    return jnp.dot(a, b, preferred_element_type=F32)
+
+
+def wait_in(ref, sem):
+    pltpu.make_async_copy(ref, ref, sem).wait()
+
+
+def layer_kernel(
+    n_st, n_tp, block_count, per_block, block_len, local_heads, seq_len, pass_rows,
+    tokens_h, store_h, ids_v, mix_gain, gv_h, gg_h, taps, channel_gain, mo_h, query_gain,
+    passage_gain, qw_h, kw_h, vw_h, ao_h, blend_gain,
+    out_ref,
+    tok, sto, gv, gg, mo, qw, kw, vw, ao, load_sem,
+    ids_all, ids_s, ids_send, ids_recv, ids_sem,
+    q_all, q_stage, q_send, q_recv,
+    k_all, v_all, k_stage, v_stage, kv_send, kv_recv,
+    gp, conv, scol, stat_all, stat_send, stat_recv, act,
+    out_o, out_s, ret_o, ret_s, o_send, o_recv, s_send, s_recv,
+    part, from_left, from_right, r_send, r_recv,
+):
+    st = lax.axis_index("st")
+    tp = lax.axis_index("tp")
+    core = lax.rem(st, 2)
+    chip = st // 2
+    n_chip = n_st // 2
+    other = 1 - core
+    T = tok.shape[0]
+    R = sto.shape[0]
+    HW = q_stage.shape[1]
+    CL = act.shape[1]
+
+    loads = []
+    for n, (a, b) in enumerate(
+        [(tokens_h, tok), (qw_h, qw), (store_h, sto), (kw_h, kw), (vw_h, vw), (gv_h, gv),
+         (gg_h, gg), (mo_h, mo), (ao_h, ao)]
+    ):
+        c = pltpu.make_async_copy(a, b, load_sem.at[n])
+        c.start()
+        loads.append(c)
+
+    barrier = pltpu.get_barrier_semaphore()
+    for i in range(1, n_st):
+        pl.semaphore_signal(barrier, inc=1, device_id={"st": lax.rem(st + i, n_st)},
+                            device_id_type=pl.DeviceIdType.MESH)
+    for i in range(1, n_tp):
+        pl.semaphore_signal(barrier, inc=1, device_id={"tp": lax.rem(tp + i, n_tp)},
+                            device_id_type=pl.DeviceIdType.MESH)
+
+    def remote(src, dst, ssem, rsem, axis, to):
+        return pltpu.make_async_remote_copy(
+            src_ref=src, dst_ref=dst, send_sem=ssem, recv_sem=rsem, device_id={axis: to},
+            device_id_type=pl.DeviceIdType.MESH)
+
+    chunk_rows = T // n_tp
+    table = [sorted(range(n_tp), key=lambda d: -abs(d - t)) for t in range(n_tp)]
+
+    def chunk_at(k):
+        d = jnp.int32(table[0][k])
+        for t in range(1, n_tp):
+            d = jnp.where(tp == t, table[t][k], d)
+        return d
+
+    chunks = [chunk_at(k) for k in range(n_tp)]
+
+    def chunk_ds(d):
+        return pl.ds(pl.multiple_of(d * chunk_rows, chunk_rows), chunk_rows)
+
+    def peers():
+        res = [(chip * 2 + other, True, 0)]
+        for j in range(1, n_chip):
+            c = lax.rem(chip + j, n_chip)
+            res.append((c * 2 + core, False, 2 * j - 1))
+            res.append((c * 2 + other, True, 2 * j))
+        return res
+
+    loads[0].wait()
+    loads[1].wait()
+    TC = 256
+    mine = pl.ds(pl.multiple_of(core * HW, HW), HW)
+    theirs = pl.ds(pl.multiple_of(other * HW, HW), HW)
+
+    def tok_chunk(i, carry):
+        rows = pl.ds(pl.multiple_of(i * TC, TC), TC)
+        x = tok[rows, :].astype(F32)
+        y = x * lax.rsqrt(jnp.mean(x * x, axis=-1, keepdims=True) + EPS)
+        qr = (y * query_gain[...]).astype(BF)
+        q_all[st, rows, :] = mm(qr, qw[:, mine]).astype(BF)
+        q_stage[rows, :] = mm(qr, qw[:, theirs]).astype(BF)
+        tok[rows, :] = (y * mix_gain[...]).astype(BF)
+        return carry
+
+    lax.fori_loop(0, T // TC, tok_chunk, 0)
+
+    pl.semaphore_wait(barrier, n_st - 1 + n_tp - 1)
+    for i in range(1, n_st):
+        remote(ids_v, ids_all.at[st], ids_send.at[i], ids_recv.at[st], "st",
+               lax.rem(st + i, n_st)).start()
+    ids_own = pltpu.make_async_copy(ids_v, ids_all.at[st], ids_recv.at[st])
+    ids_own.start()
+
+    def q_copies(k):
+        rows = chunk_ds(chunks[k])
+        for to, stage, n in peers():
+            src = q_stage.at[rows] if stage else q_all.at[st, rows]
+            yield remote(src, q_all.at[st, rows], q_send.at[n, k], q_recv.at[st, k], "st", to)
+
+    for k in range(n_tp):
+        for c in q_copies(k):
+            c.start()
+
+    for n in range(2, 5):
+        loads[n].wait()
+    RC = 256
+    n_rc = R // RC
+    RP = RC // pass_rows
+    pass_local = R // pass_rows
+    partner = chip * 2 + other
+
+    def store_chunk(i, carry):
+        rows = pl.ds(pl.multiple_of(i * RC, RC), RC)
+        x = sto[rows, :].astype(F32)
+        n = (x * lax.rsqrt(jnp.mean(x * x, axis=-1, keepdims=True) + EPS) * passage_gain[...]).astype(BF)
+        here, slots = pl.ds(i * RP, RP), pl.ds(core * pass_local + i * RP, RP)
+        k_stage[here] = mm(n, kw[:, theirs]).astype(BF).reshape(RP, pass_rows, HW)
+        v_stage[here] = mm(n, vw[:, theirs]).astype(BF).reshape(RP, pass_rows, HW)
+        remote(k_stage.at[here], k_all.at[slots], kv_send.at[0, i], kv_recv.at[0, i], "st", partner).start()
+        remote(v_stage.at[here], v_all.at[slots], kv_send.at[1, i], kv_recv.at[1, i], "st", partner).start()
+        k_all[slots] = mm(n, kw[:, mine]).astype(BF).reshape(RP, pass_rows, HW)
+        v_all[slots] = mm(n, vw[:, mine]).astype(BF).reshape(RP, pass_rows, HW)
+        return carry
+
+    lax.fori_loop(0, n_rc, store_chunk, 0)
+
+    ids_own.wait()
+    for i in range(1, n_st):
+        r = lax.rem(st + i, n_st)
+        remote(ids_v, ids_all.at[r], ids_send.at[i], ids_recv.at[r], "st", r).wait_recv()
+    c = pltpu.make_async_copy(ids_all, ids_s, ids_sem)
+    c.start()
+    c.wait()
+
+    def kv_wait(i, carry):
+        here, slots = pl.ds(i * RP, RP), pl.ds(other * pass_local + i * RP, RP)
+        remote(k_stage.at[here], k_all.at[slots], kv_send.at[0, i], kv_recv.at[0, i], "st", partner).wait()
+        remote(v_stage.at[here], v_all.at[slots], kv_send.at[1, i], kv_recv.at[1, i], "st", partner).wait()
+        return carry
+
+    lax.fori_loop(0, n_rc, kv_wait, 0)
+
+    heads = local_heads // 2
+    HD_ = HW // heads
+    per_chip = 2 * pass_local
+    chunk_blocks = block_count // n_tp
+    clane = lax.broadcasted_iota(jnp.int32, (chunk_rows, 128), 1)
+    scale = HD_ ** (-0.5)
+
+    def order(i):
+        return lax.rem(chip + 1 + i // 2, n_chip) * 2 + lax.rem(core + 1 - i % 2, 2)
+
+    def answer_copies(k, r):
+        rows = chunk_ds(chunks[k])
+        return (
+            remote(out_o.at[r, rows], ret_o.at[st, rows], o_send.at[r, k], o_recv.at[st, k], "st", r),
+            remote(out_s.at[r, k], ret_s.at[st, k], s_send.at[r, k], s_recv.at[st, k], "st", r),
+        )
+
+    def attend(k):
+        d = chunks[k]
+        rows = chunk_ds(d)
+
+        def one(i, carry):
+            r = order(i)
+
+            @pl.when(i < n_st - 1)
+            def _():
+                remote(q_all.at[st, rows], q_all.at[r, rows], q_send.at[0, k], q_recv.at[r, k], "st", r).wait_recv()
+
+            stats = jnp.zeros((chunk_rows, 128), F32)
+            for h in range(heads):
+                cols = slice(h * HD_, (h + 1) * HD_)
+                tops, dens = [], []
+                for u in range(chunk_blocks):
+                    b = d * chunk_blocks + u
+                    brow = pl.ds(pl.multiple_of(b * block_len, block_len), block_len)
+                    q = q_all[r, brow, cols]
+                    ks, vs, bias = [], [], []
+                    for j in range(per_block):
+                        p = ids_s[r, b, j] - chip * per_chip
+                        spread_p = jnp.full((1, pass_rows), p, jnp.int32)
+                        valid = jnp.logical_and(spread_p >= 0, spread_p < per_chip)
+                        bias.append(jnp.where(valid, 0.0, NEG))
+                        slot = jnp.clip(p, 0, per_chip - 1)
+                        ks.append(k_all[slot][:, cols])
+                        vs.append(v_all[slot][:, cols])
+                    s = lax.dot_general(q, jnp.concatenate(ks, axis=0), (((1,), (1,)), ((), ())),
+                                        preferred_element_type=F32)
+                    s = s * scale + jnp.concatenate(bias, axis=1)
+                    top = jnp.maximum(jnp.max(s, axis=1, keepdims=True), NEG / 2)
+                    e = jnp.exp(s - top)
+                    dens.append(jnp.sum(e, axis=1, keepdims=True))
+                    tops.append(top)
+                    out_o[r, brow, cols] = mm(e.astype(BF), jnp.concatenate(vs, axis=0)).astype(BF)
+                stats = jnp.where(clane == 2 * h, jnp.concatenate(tops, axis=0), stats)
+                stats = jnp.where(clane == 2 * h + 1, jnp.concatenate(dens, axis=0), stats)
+            out_s[r, k] = jnp.transpose(stats)[:8]
+
+            @pl.when(i < n_st - 1)
+            def _():
+                for c in answer_copies(k, r):
+                    c.start()
+
+            return carry
+
+        lax.fori_loop(0, n_st, one, 0)
+
+    attend(0)
+
+    loads[5].wait()
+    loads[6].wait()
+    per_seq = seq_len
+    pad = (gp.shape[1] - per_seq) // 2
+    gp[:, :pad] = jnp.zeros((gp.shape[0], pad, CL), F32)
+    gp[:, pad + per_seq:] = jnp.zeros((gp.shape[0], pad, CL), F32)
+
+    def glu_chunk(i, carry):
+        mr = tok[pl.ds(pl.multiple_of(i * TC, TC), TC), :]
+        gated = (mm(mr, gv[...]) * jax.nn.sigmoid(mm(mr, gg[...]))).astype(BF).astype(F32)
+        for u in range(TC // per_seq):
+            gp[i * (TC // per_seq) + u, pad:pad + per_seq, :] = gated[u * per_seq:(u + 1) * per_seq]
+        return carry
+
+    lax.fori_loop(0, T // TC, glu_chunk, 0)
+    tap_values = taps[...].astype(F32)
+    n_tap = taps.shape[0]
+    lead = pad - (n_tap - 1) // 2
+    CC = 32
+    per = per_seq // CC
+    lane = lax.broadcasted_iota(jnp.int32, (CC, 128), 1)
+
+    def conv_chunk(i, carry):
+        seq = i // per
+        base = pl.multiple_of(lax.rem(i, per) * CC, CC)
+        win = gp[seq, pl.ds(base, CC + 2 * pad), :]
+        acc = jnp.zeros((CC, CL), F32)
+        for k in range(n_tap):
+            acc = acc + win[lead + k:lead + k + CC] * tap_values[k:k + 1]
+        rows = pl.ds(pl.multiple_of(i * CC, CC), CC)
+        conv[rows, :] = acc
+        s = jnp.sum(acc, axis=1, keepdims=True)
+        ss = jnp.sum(acc * acc, axis=1, keepdims=True)
+        scol[rows, :] = jnp.where(lane == 0, s, jnp.where(lane == 1, ss, 0.0))
+        return carry
+
+    lax.fori_loop(0, T // CC, conv_chunk, 0)
+    stat_all[tp] = jnp.transpose(scol[...])[:8]
+    for i in range(1, n_tp):
+        remote(stat_all.at[tp], stat_all.at[tp], stat_send.at[i], stat_recv.at[tp], "tp",
+               lax.rem(tp + i, n_tp)).start()
+
+    attend(1)
+
+    total = stat_all[tp]
+    for i in range(1, n_tp):
+        r = lax.rem(tp + i, n_tp)
+        remote(stat_all.at[tp], stat_all.at[r], stat_send.at[i], stat_recv.at[r], "tp", r).wait_recv()
+        total = total + stat_all[r]
+    ca = CL * n_tp
+    mean = total / ca
+    spread = jnp.transpose(jnp.concatenate([mean, jnp.zeros((120, T), F32)], axis=0))
+    row_mean = spread[:, 0:1]
+    inv = lax.rsqrt(spread[:, 1:2] - row_mean * row_mean + EPS)
+    a = (conv[...] - row_mean) * inv * channel_gain[...]
+    act[...] = (a / (1.0 + jnp.exp(-a))).astype(BF)
+    loads[7].wait()
+    loads[8].wait()
+
+    SUB = 4
+    SR = chunk_rows // SUB
+
+    def hop(k, u, ahead, buf, way):
+        d = chunks[k]
+        prow = pl.ds(pl.multiple_of(d * chunk_rows + u * SR, SR), SR)
+        brow = pl.ds(u * SR, SR)
+        to = jnp.clip(tp + ahead, 0, n_tp - 1)
+        return prow, brow, remote(part.at[prow], buf.at[d, brow], r_send.at[way, d, u],
+                                  r_recv.at[way, d, u], "tp", to)
+
+    ways = ((1, from_left, 0), (-1, from_right, 1))
+
+    def goes(k, way):
+        return tp < chunks[k] if way == 0 else tp > chunks[k]
+
+    def at_end(way):
+        return tp == 0 if way == 0 else tp == n_tp - 1
+
+    def finish(k):
+        rows = chunk_ds(chunks[k])
+        for i in range(n_st - 1):
+            r = order(i)
+            remote(out_o.at[r, rows], ret_o.at[r, rows], o_send.at[r, k], o_recv.at[r, k], "st", r).wait_recv()
+            remote(out_s.at[r, k], ret_s.at[r, k], s_send.at[r, k], s_recv.at[r, k], "st", r).wait_recv()
+        ret_o[st, rows, :] = out_o[st, rows, :]
+        ret_s[st, k] = out_s[st, k]
+        stats = jnp.transpose(jnp.concatenate(
+            [ret_s[c, k] for c in range(n_st)] + [jnp.zeros((128 - 8 * n_st, chunk_rows), F32)], axis=0))
+        pieces = []
+        for g in range(2):
+            for h in range(heads):
+                cols = slice(h * HD_, (h + 1) * HD_)
+                at = [8 * (c * 2 + g) + 2 * h for c in range(n_chip)]
+                best = functools.reduce(jnp.maximum, [stats[:, x:x + 1] for x in at])
+                num, den = 0.0, 0.0
+                for c in range(n_chip):
+                    w = jnp.exp(stats[:, at[c]:at[c] + 1] - best)
+                    num = num + w * ret_o[c * 2 + g, rows, cols].astype(F32)
+                    den = den + w * stats[:, at[c] + 1:at[c] + 2]
+                pieces.append((num / den).astype(BF))
+        attended = jnp.concatenate(pieces, axis=1)
+        act_rows = act[rows, :]
+        NC = 512
+        for i in range(part.shape[1] // NC):
+            cols = slice(i * NC, (i + 1) * NC)
+            value = mm(act_rows, mo[:, cols]) + blend_gain[:, cols] * mm(attended, ao[:, cols])
+            part[rows, cols] = value.astype(BF)
+        if k < n_tp - 1:
+            for ahead, buf, way in ways:
+                @pl.when(jnp.logical_and(goes(k, way), at_end(way)))
+                def _(ahead=ahead, buf=buf, way=way):
+                    for u in range(SUB):
+                        hop(k, u, ahead, buf, way)[2].start()
+
+    def forward(k, u):
+        for ahead, buf, way in ways:
+            @pl.when(jnp.logical_and(goes(k, way), jnp.logical_not(at_end(way))))
+            def _(ahead=ahead, buf=buf, way=way):
+                prow, brow, copy = hop(k, u, ahead, buf, way)
+                copy.wait_recv()
+                part[prow, :] = (part[prow, :].astype(F32) + buf[chunks[k], brow, :].astype(F32)).astype(BF)
+                copy.start()
+
+    forwarded = 0
+    for k in range(n_tp):
+        finish(k)
+        if k + 2 < n_tp:
+            attend(k + 2)
+        elif k < n_tp - 1:
+            for u in range(SUB):
+                forward(k - 2, u)
+            forwarded = k - 1
+    for u in range(SUB):
+        for k in range(forwarded, n_tp - 1):
+            forward(k, u)
+
+    for u in range(SUB):
+        prow = pl.ds(pl.multiple_of(tp * chunk_rows + u * SR, SR), SR)
+        brow = pl.ds(u * SR, SR)
+
+        for ahead, buf, way in ways:
+            @pl.when(jnp.logical_not(at_end(way)))
+            def _(buf=buf, way=way, ahead=ahead):
+                to = jnp.clip(tp - ahead, 0, n_tp - 1)
+                remote(part.at[prow], buf.at[tp, brow], r_send.at[way, tp, u], r_recv.at[way, tp, u], "tp",
+                       to).wait_recv()
+
+            @pl.when(at_end(way))
+            def _(buf=buf):
+                buf[tp, brow, :] = jnp.zeros((SR, part.shape[1]), BF)
+
+        out_ref[brow, :] = (
+            part[prow, :].astype(F32) + from_left[tp, brow, :].astype(F32) + from_right[tp, brow, :].astype(F32)
+        ).astype(BF)
+
+    for i in range(1, n_st):
+        r = lax.rem(st + i, n_st)
+        remote(ids_v, ids_all.at[st], ids_send.at[i], ids_recv.at[st], "st", r).wait_send()
+    for k in range(n_tp):
+        for c in q_copies(k):
+            c.wait_send()
+        for i in range(n_st - 1):
+            for c in answer_copies(k, order(i)):
+                c.wait_send()
+    for i in range(1, n_tp):
+        remote(stat_all.at[tp], stat_all.at[tp], stat_send.at[i], stat_recv.at[tp], "tp",
+               lax.rem(tp + i, n_tp)).wait_send()
+    for k in range(n_tp - 1):
+        for ahead, buf, way in ways:
+            @pl.when(goes(k, way))
+            def _(ahead=ahead, buf=buf, way=way):
+                for u in range(SUB):
+                    hop(k, u, ahead, buf, way)[2].wait_send()
+
+
+def fused_local(
+    tokens, store, passage_ids, mix_gain, glu_value, glu_gate, conv_taps, channel_gain, mix_out,
+    query_gain, passage_gain, query_proj, key_proj, value_proj, attn_out, blend_gain,
+):
+    n_st = lax.axis_size("st")
+    n_tp = lax.axis_size("tp")
+    T, D = tokens.shape
+    P_, PR, _ = store.shape
+    R = P_ * PR
+    W = query_proj.shape[1]
+    HW = W // 2
+    CL = glu_value.shape[1]
+    nb, per_block = passage_ids.shape
+    ids = jnp.pad(passage_ids, ((0, 0), (0, 128 - per_block)))
+    pad = 8 * pl.cdiv((conv_taps.shape[0] - 1) // 2, 8)
+    DMA = pltpu.SemaphoreType.DMA
+    V = pltpu.VMEM
+    SUB = 4
+    kern = functools.partial(layer_kernel, n_st, n_tp, nb, per_block, T // nb, W // HD, SEQ_LEN, PR)
+    hbm = pl.BlockSpec(memory_space=pl.ANY)
+    vm = pl.BlockSpec(memory_space=pltpu.VMEM)
+    return pl.pallas_call(
+        kern,
+        out_shape=jax.ShapeDtypeStruct((T // n_tp, D), BF),
+        in_specs=[hbm, hbm, vm, vm, hbm, hbm, vm, vm, hbm, vm, vm, hbm, hbm, hbm, hbm, vm],
+        out_specs=vm,
+        scratch_shapes=[
+            V((T, D), BF), V((R, D), BF), V((D, CL), BF), V((D, CL), BF), V((CL, D), BF),
+            V((D, W), BF), V((D, W), BF), V((D, W), BF), V((W, D), BF), DMA((9,)),
+            V((n_st, nb, 128), jnp.int32), pltpu.SMEM((n_st, nb, 128), jnp.int32),
+            DMA((n_st,)), DMA((n_st,)), DMA,
+            V((n_st, T, HW), BF), V((T, HW), BF), DMA((n_st - 1, n_tp)), DMA((n_st, n_tp)),
+            V((2 * P_, PR, HW), BF), V((2 * P_, PR, HW), BF), V((P_, PR, HW), BF), V((P_, PR, HW), BF),
+            DMA((2, R // 256)), DMA((2, R // 256)),
+            V((T // SEQ_LEN, SEQ_LEN + 2 * pad, CL), F32), V((T, CL), F32), V((T, 128), F32),
+            V((n_tp, 8, T), F32), DMA((n_tp,)), DMA((n_tp,)), V((T, CL), BF),
+            V((n_st, T, HW), BF), V((n_st, n_tp, 8, T // n_tp), F32), V((n_st, T, HW), BF),
+            V((n_st, n_tp, 8, T // n_tp), F32),
+            DMA((n_st, n_tp)), DMA((n_st, n_tp)), DMA((n_st, n_tp)), DMA((n_st, n_tp)),
+            V((T, D), BF), V((n_tp, T // n_tp, D), BF), V((n_tp, T // n_tp, D), BF),
+            DMA((2, n_tp, SUB)), DMA((2, n_tp, SUB)),
+        ],
+        compiler_params=pltpu.CompilerParams(
+            collective_id=0, has_side_effects=True, vmem_limit_bytes=60 * 1024 * 1024),
+        name="layer",
+    )(
+        tokens, store.reshape(R, D), ids, mix_gain.reshape(1, D), glu_value, glu_gate, conv_taps,
+        channel_gain.reshape(1, CL), mix_out, query_gain.reshape(1, D), passage_gain.reshape(1, D),
+        query_proj, key_proj, value_proj, attn_out, blend_gain.reshape(1, D),
+    )
+
+
 def solution(mesh):
     in_specs = (
         P(("grp", "st"), None),
@@ -224,4 +678,9 @@
         P(),
     )
     out_specs = P(("grp", "st", "tp"), None)
-    return jax.shard_map(local, mesh=mesh, in_specs=in_specs, out_specs=out_specs, check_vma=False)
+    def body(*args):
+        even = args[11].shape[1] // HD % 2 == 0 and mesh.shape["st"] % 2 == 0
+        even = even and args[2].shape[0] % mesh.shape["tp"] == 0 and mesh.shape["st"] <= 16
+        return (fused_local if even else local)(*args)
+
+    return jax.shard_map(body, mesh=mesh, in_specs=in_specs, out_specs=out_specs, check_vma=False)

time: 270 us -> 70 us (0.26)
  local copies, waits for them, and re-layouts: 94.7 us -> 3.24 us
  Pallas kernels: 0 us -> 66.5 us
  waiting for transfers between devices: 65.9 us -> 0 us
  matrix products: 41 us -> 0 us
  starting transfers between devices: 21.2 us -> 0 us
  other arithmetic: 19.6 us -> 0 us
  between operations: 13.8 us -> 0.01 us
  blocking collectives: 12.7 us -> 0 us
    pallas_call x0 -> x1, Pallas kernels: none -> 66.5 us  [fused_local(): pl.pallas_call(kern, out_shape=jax.ShapeDtypeStruct((T // n_tp, D), BF),...]
    reduce_scatter x1 -> x0, waiting for transfers between devices: 44.7 us -> none  [local(): lax.psum_scatter((conv_term + blend_gain * attn_term).astype(jnp.bfloat16...]
    dot_general x10 -> x0, matrix products: 41 us -> none  [the longest x1 10.1 us: passage_attention(): jnp.einsum('ghqr,grhd->gqhd', weights, value_heads, preferred_element_typ...]
    slice x3 -> x0, local copies, waits for them, and re-layouts: 35.3 us -> none  [the longest x2 23.5 us: passage_attention(): keys_values[:, :, span_width:]]
    all_to_all x5 -> x0, waiting for transfers between devices: 21.1 us -> none  [the longest x1 21.1 us: local(): lax.all_to_all(answer_out.reshape(owners, capacity, block_len, head_width...]
    all_to_all x5 -> x0, starting transfers between devices: 21.1 us -> none  [the longest x1 5.08 us: local(): lax.all_to_all(answer_out.reshape(owners, capacity, block_len, head_width...]
    another operation x2 -> x0, local copies, waits for them, and re-layouts: 14.5 us -> none  [the longest x1 7.6 us: local(): answer_out.reshape(owners, capacity, block_len, head_width)]
    gather x4 -> x0, local copies, waits for them, and re-layouts: 14.3 us -> none  [the longest x1 8.92 us: local(): served = memory[asked.reshape(owners * capacity)]]
  transfers between devices with their start and end apart: 6 -> 0, of which waited for: 2 -> 0; matrix products, arithmetic and copies ran while one was open for 45% -> 0% of each run, Pallas kernels for 0% -> 0%
where the time goes in v2:
time: 70 us; the launch traced here: 69.8 us
  Pallas kernels  66.5 us (95%)
  local copies, waits for them, and re-layouts  3.24 us (5%)
    pallas_call x1, Pallas kernels, fused_local(): pl.pallas_call(kern, out_shape=jax.ShapeDtypeStruct((T // n_tp, D), BF),...  66.5 us
    unnamed x2, local copies, waits for them, and re-layouts  2.64 us

profile of v2, /device:TPU:0, one launch (start us, length us, event | category | flops | bytes accessed | tf_op | source)
XLA Modules:
  0.0 69.8 jit_solution(12403992791583648535)
XLA Ops:
  0.0 0.8 %copy.17 = s32[8,4]{1,0:T(8,128)S(1)} copy(s32[8,4]{0,1:T(4,128)} %param.18) | data formatting | bytes 256 | tf_op args[2]
  0.8 0.6 pad.4.ids_v
  1.4 66.5 %layer.1 = bf16[128,2048]{1,0:T(8,128)(2,1)} custom-call(bf16[512,2048]{1,0:T(8,128)(2,1)} %tokens_h.1, bf16[1024,2048]{1,0:T(8,128)(2,1)} %bitcast.6, s32[8,128]{1,0:T(8,128)} %pad.4.ids_v, f32[1,2048]{1,0:T(1,128)} %bitcast.7, bf16[2048,256]{1,0:T(8,128)(2,1)} %gv_h.1, bf16[2048,256]{1,0:T(8,128)(2,1)} %gg_h.1, bf16[31,256]{1,0:T(8,128)(2,1)} %taps.1, ...), custom_call_target="tpu_custom_call" | custom-call | tf_op jit(solution)/shard_map/layer/pallas_call | solution.py:630
  67.9 1.9 %copy.19 = bf16[128,2048]{1,0:T(8,128)(2,1)} copy(bf16[128,2048]{1,0:T(8,128)(2,1)} %layer.1) | data formatting | bytes 1048576

commit v3 on v2

--- a/solution.py
+++ b/solution.py
@@ -326,7 +326,7 @@
 
     for n in range(2, 5):
         loads[n].wait()
-    RC = 256
+    RC = 512
     n_rc = R // RC
     RP = RC // pass_rows
     pass_local = R // pass_rows
@@ -449,7 +449,7 @@
     tap_values = taps[...].astype(F32)
     n_tap = taps.shape[0]
     lead = pad - (n_tap - 1) // 2
-    CC = 32
+    CC = 64
     per = per_seq // CC
     lane = lax.broadcasted_iota(jnp.int32, (CC, 128), 1)
 
@@ -457,9 +457,17 @@
         seq = i // per
         base = pl.multiple_of(lax.rem(i, per) * CC, CC)
         win = gp[seq, pl.ds(base, CC + 2 * pad), :]
-        acc = jnp.zeros((CC, CL), F32)
-        for k in range(n_tap):
-            acc = acc + win[lead + k:lead + k + CC] * tap_values[k:k + 1]
+        acc = None
+        for res in range(8):
+            group = None
+            for k in range(n_tap):
+                if (lead + k) % 8 == res:
+                    at = lead + k - res
+                    term = win[at:at + CC + (8 if res else 0)] * tap_values[k:k + 1]
+                    group = term if group is None else group + term
+            if group is not None:
+                group = group[res:res + CC]
+                acc = group if acc is None else acc + group
         rows = pl.ds(pl.multiple_of(i * CC, CC), CC)
         conv[rows, :] = acc
         s = jnp.sum(acc, axis=1, keepdims=True)
@@ -639,7 +647,7 @@
             DMA((n_st,)), DMA((n_st,)), DMA,
             V((n_st, T, HW), BF), V((T, HW), BF), DMA((n_st - 1, n_tp)), DMA((n_st, n_tp)),
             V((2 * P_, PR, HW), BF), V((2 * P_, PR, HW), BF), V((P_, PR, HW), BF), V((P_, PR, HW), BF),
-            DMA((2, R // 256)), DMA((2, R // 256)),
+            DMA((2, R // 512)), DMA((2, R // 512)),
             V((T // SEQ_LEN, SEQ_LEN + 2 * pad, CL), F32), V((T, CL), F32), V((T, 128), F32),
             V((n_tp, 8, T), F32), DMA((n_tp,)), DMA((n_tp,)), V((T, CL), BF),
             V((n_st, T, HW), BF), V((n_st, n_tp, 8, T // n_tp), F32), V((n_st, T, HW), BF),

time: 70 us -> 66.9 us (0.956)
  Pallas kernels: 66.5 us -> 63.4 us
    pallas_call x1, Pallas kernels: 66.5 us -> 63.4 us  [fused_local(): pl.pallas_call(kern, out_shape=jax.ShapeDtypeStruct((T // n_tp, D), BF),...]
where the time goes in v3:
time: 66.9 us; the launch traced here: 66.6 us
  Pallas kernels  63.4 us (95%)
  local copies, waits for them, and re-layouts  3.24 us (5%)
    pallas_call x1, Pallas kernels, fused_local(): pl.pallas_call(kern, out_shape=jax.ShapeDtypeStruct((T // n_tp, D), BF),...  63.4 us
    unnamed x2, local copies, waits for them, and re-layouts  2.64 us

profile of v3, /device:TPU:0, one launch (start us, length us, event | category | flops | bytes accessed | tf_op | source)
XLA Modules:
  0.0 66.6 jit_solution(13359502207954797918)
XLA Ops:
  0.0 0.8 %copy.17 = s32[8,4]{1,0:T(8,128)S(1)} copy(s32[8,4]{0,1:T(4,128)} %param.18) | data formatting | bytes 256 | tf_op args[2]
  0.8 0.6 pad.4.ids_v
  1.4 63.4 %layer.1 = bf16[128,2048]{1,0:T(8,128)(2,1)} custom-call(bf16[512,2048]{1,0:T(8,128)(2,1)} %tokens_h.1, bf16[1024,2048]{1,0:T(8,128)(2,1)} %bitcast.6, s32[8,128]{1,0:T(8,128)} %pad.4.ids_v, f32[1,2048]{1,0:T(1,128)} %bitcast.7, bf16[2048,256]{1,0:T(8,128)(2,1)} %gv_h.1, bf16[2048,256]{1,0:T(8,128)(2,1)} %gg_h.1, bf16[31,256]{1,0:T(8,128)(2,1)} %taps.1, ...), custom_call_target="tpu_custom_call" | custom-call | tf_op jit(solution)/shard_map/layer/pallas_call | solution.py:638
  64.7 1.9 %copy.19 = bf16[128,2048]{1,0:T(8,128)(2,1)} copy(bf16[128,2048]{1,0:T(8,128)(2,1)} %layer.1) | data formatting | bytes 1048576
